TPU v7x, 32 devices: a whole 2x2x4 slice. The times are simulated.
32 devices in a mesh: sp: 16 (over z, y, x), tp: 2 (over core).
Axes of the slice: x: 2, y: 2, z: 4, core: 2. Of those that a mesh axis runs over, the one named last changes fastest.
Arguments:
- query_logits: bfloat16 [2048, 1024], P('sp', 'tp'), may hold values from -6 to 6
- value_rows: bfloat16 [2048, 1024], P('sp', 'tp'), may hold values from -6 to 6
- onward_forget_logits: bfloat16 [2048, 1024], P('sp', 'tp'), may hold values from -5.5 to 5.5
- reverse_forget_logits: bfloat16 [2048, 1024], P('sp', 'tp'), may hold values from -5.5 to 5.5
- output_gate_logits: bfloat16 [2048, 1024], P('sp', 'tp'), may hold values from -6 to 6
- onward_floor_gap: float32 [1024], P('tp'), may hold values from 0 to 0.12, as said below
- reverse_floor_gap: float32 [1024], P('tp'), may hold values from 0 to 0.12, as said below
- extra_log_decay: float32 [2048, 8], P('sp', 'tp'), may hold values from -2.1 to 0
- per_head_gain: float32 [128], replicated, may hold values from 0.1 to 1.9
- residual: bfloat16 [2048, 2048], P('sp', 'tp'), may hold values from -8 to 8
- output_matrix: bfloat16 [1024, 2048], P(None, 'tp'), may hold values from -0.375 to 0.375
- inner_norm_gain: float32 [2048], P('tp'), may hold values from 0.1 to 1.9
- inner_norm_bias: float32 [2048], P('tp'), may hold values from -1.5 to 1.5
- gate_matrix: bfloat16 [2048, 5632], P('sp', 'tp'), may hold values from -0.125 to 0.125
- up_matrix: bfloat16 [2048, 5632], P('sp', 'tp'), may hold values from -0.125 to 0.125
- down_matrix: bfloat16 [5632, 2048], P('tp', 'sp'), may hold values from -0.15625 to 0.15625
- closing_norm_gain: float32 [2048], P('tp'), may hold values from 0.1 to 1.9
- closing_norm_bias: float32 [2048], P('tp'), may hold values from -1.5 to 1.5
Outputs:
- layer_output: bfloat16 [2048, 2048], P('sp', 'tp')
Inputs may be any that keep to these rules, and one draw needn't show every extreme that they name: `onward_floor_gap`: positive. `reverse_floor_gap`: positive.
All inputs are finite; a program needn't handle non-finite values.
Results may differ from a plain program's by a relative error of at most 0.014.
Values may be sent and summed in bfloat16 or wider, within the bound.
A program may use at most 128 MiB of HBM per device.

v0:
```python
import math
import jax
import jax.numpy as jnp
from jax import lax
from jax.sharding import PartitionSpec as P

D = 2048
highest_precision = lax.Precision.HIGHEST
alpha_mix = 2.0**0.25
norm_eps = 1e-05
head_eps = 1e-06


def prefix(x, axis, join, neutral, backward):
    count = lax.axis_size(axis)
    place = lax.axis_index(axis)
    ahead = count - 1 - place if backward else place
    gathered = jax.tree.map(
        lambda a, kind: lax.all_gather(a.astype(kind), axis), x, (jnp.bfloat16, jnp.bfloat16)
    )
    state = jax.tree.map(lambda a, e: jnp.zeros_like(a) + jnp.asarray(e, a.dtype), x, neutral)

    def one(step, state):
        source = count - 1 - step if backward else step
        return join(
            state,
            jax.tree.map(
                lambda a, own: lax.dynamic_index_in_dim(a, source, 0, False).astype(own.dtype),
                gathered,
                x,
            ),
        )

    return lax.fori_loop(0, ahead, one, state)


def decay_factors(unscaled_input, lower_bound_gap, extra_decays):
    decay_factor = lower_bound_gap * jax.nn.sigmoid(-unscaled_input.astype(jnp.float32))
    return (jnp.log1p(-decay_factor) + extra_decays, decay_factor)


def local_pass(query, keys, values, log_decay):
    rows, head_count, model_width = query.shape
    span = math.gcd(rows, 128)
    count = rows // span
    triangle = jnp.tril(jnp.ones((span, span), jnp.float32))

    def blocks(array):
        return array.reshape(count, span, head_count, array.shape[2])

    def advance(carry, inputs):
        running_state, offset = carry
        query_block, key_block, value_tile, log_block = inputs
        running = jnp.cumsum(log_block, axis=0)
        final_index = running[-1]
        decayed_query = query_block * jnp.exp(running)
        key_inverse = key_block * jnp.exp(-running)
        key_stop = key_block * jnp.exp(final_index[None] - running)
        scores = (
            jnp.einsum("thk,shk->hts", decayed_query, key_inverse, precision=highest_precision)
            * triangle[None]
        )
        inner = jnp.einsum("hts,shv->thv", scores, value_tile, precision=highest_precision)
        carried_state = jnp.einsum(
            "nex,exl->nel", decayed_query, running_state, precision=highest_precision
        )
        query_start = decayed_query * jnp.exp(offset)[None]
        running_state = jnp.exp(final_index)[:, :, None] * running_state + jnp.einsum(
            "ojy,oje->jye", key_stop, value_tile, precision=highest_precision
        )
        return ((running_state, offset + final_index), (inner + carried_state, query_start))

    start = (
        jnp.zeros((head_count, model_width, values.shape[2]), jnp.float32),
        jnp.zeros((head_count, model_width), jnp.float32),
    )
    final, outputs = lax.scan(
        advance, start, (blocks(query), blocks(keys), blocks(values), blocks(log_decay))
    )
    result = outputs[0].reshape(rows, head_count, values.shape[2])
    query_start = outputs[1].reshape(rows, head_count, model_width)
    return (result, query_start, final[1], final[0])


def join(earlier, later):
    return (earlier[0] + later[0], jnp.exp(later[0])[:, :, None] * earlier[1] + later[1])


def row_norm(before, moments, gain, bias):
    mean = moments[0] / D
    spread = moments[1] / D - mean * mean
    return (before - mean[:, None]) * lax.rsqrt(spread + norm_eps)[:, None] * gain + bias


def shards(
    query_logits,
    value_rows,
    onward_forget_logits,
    reverse_forget_logits,
    output_gate_logits,
    onward_floor_gap,
    reverse_floor_gap,
    extra_log_decay,
    per_head_gain,
    residual,
    output_matrix,
    inner_norm_gain,
    inner_norm_bias,
    gate_matrix,
    up_matrix,
    down_matrix,
    closing_norm_gain,
    closing_norm_bias,
):
    gate_whole, up_whole, down_whole = (
        lax.all_gather(gate_matrix, "sp", axis=0, tiled=True),
        lax.all_gather(up_matrix, "sp", axis=0, tiled=True),
        lax.all_gather(down_matrix, "sp", axis=1, tiled=True),
    )
    rows = query_logits.shape[0]
    head_count = extra_log_decay.shape[1]
    model_width = query_logits.shape[1] // head_count
    shape_head = (rows, head_count, model_width)
    query = jax.nn.silu(query_logits.astype(jnp.float32)).reshape(shape_head)
    values = value_rows.astype(jnp.float32).reshape(shape_head)
    extra_decays = jnp.repeat(extra_log_decay, model_width, axis=1)
    onward_log_decay, onward_key_rows = decay_factors(
        onward_forget_logits, onward_floor_gap, extra_decays
    )
    reverse_log_decay, reverse_key_rows = decay_factors(
        reverse_forget_logits, reverse_floor_gap, extra_decays
    )
    empty_total = jnp.zeros((head_count, model_width), jnp.float32)
    empty_state = jnp.zeros((head_count, model_width, model_width), jnp.float32)
    upcoming_part, upcoming_begin, ahead_total, ahead_state = local_pass(
        query, onward_key_rows.reshape(shape_head), values, onward_log_decay.reshape(shape_head)
    )
    incoming_state = prefix(
        (ahead_total, ahead_state), "sp", join, (empty_total, empty_state), False
    )
    upcoming_part = upcoming_part + jnp.einsum(
        "nex,exl->nel", upcoming_begin, incoming_state[1], precision=highest_precision
    )
    preceding_part, preceding_begin, behind_total, behind_state = local_pass(
        jnp.flip(query, axis=0),
        jnp.flip(reverse_key_rows.reshape(shape_head), axis=0),
        jnp.flip(values, axis=0),
        jnp.flip(reverse_log_decay.reshape(shape_head), axis=0),
    )
    arriving_state = prefix(
        (behind_total, behind_state), "sp", join, (empty_total, empty_state), True
    )
    preceding_part = jnp.flip(
        preceding_part
        + jnp.einsum(
            "nex,exl->nel", preceding_begin, arriving_state[1], precision=highest_precision
        ),
        axis=0,
    )
    mixed = upcoming_part + preceding_part
    normed = (
        mixed * lax.rsqrt(jnp.mean(mixed * mixed, axis=2, keepdims=True) + head_eps) * per_head_gain
    )
    gated = (
        normed.reshape(rows, head_count * model_width)
        * jax.nn.silu(output_gate_logits.astype(jnp.float32))
    ).astype(jnp.bfloat16)
    mixer = jnp.dot(
        lax.all_gather(gated, "tp", axis=1, tiled=True),
        output_matrix,
        preferred_element_type=jnp.float32,
    )
    before_middle = alpha_mix * residual.astype(jnp.float32) + mixer
    moments = lax.psum(
        (jnp.sum(before_middle, axis=1), jnp.sum(before_middle * before_middle, axis=1)), "tp"
    )
    middle = row_norm(before_middle, moments, inner_norm_gain, inner_norm_bias).astype(jnp.bfloat16)
    whole = lax.all_gather(middle, "tp", axis=1, tiled=True)
    gate = jnp.dot(whole, gate_whole, preferred_element_type=jnp.float32)
    up = jnp.dot(whole, up_whole, preferred_element_type=jnp.float32)
    hidden = (jax.nn.silu(gate) * up).astype(jnp.bfloat16)
    partial_value = jnp.dot(hidden, down_whole, preferred_element_type=jnp.float32)
    feed = lax.psum_scatter(
        partial_value.astype(jnp.bfloat16), "tp", scatter_dimension=1, tiled=True
    ).astype(jnp.float32)
    before_final = alpha_mix * middle.astype(jnp.float32) + feed
    closing = lax.psum(
        (jnp.sum(before_final, axis=1), jnp.sum(before_final * before_final, axis=1)), "tp"
    )
    return row_norm(before_final, closing, closing_norm_gain, closing_norm_bias).astype(
        jnp.bfloat16
    )


def solution(mesh):
    placed = (
        P("sp", "tp"),
        P("sp", "tp"),
        P("sp", "tp"),
        P("sp", "tp"),
        P("sp", "tp"),
        P("tp"),
        P("tp"),
        P("sp", "tp"),
        P(),
        P("sp", "tp"),
        P(None, "tp"),
        P("tp"),
        P("tp"),
        P("sp", "tp"),
        P("sp", "tp"),
        P("tp", "sp"),
        P("tp"),
        P("tp"),
    )
    return jax.shard_map(
        shards, mesh=mesh, in_specs=placed, out_specs=P("sp", "tp"), check_vma=False
    )
```

profile of v0, /device:TPU:0, one launch (start us, length us, event | category | flops | bytes accessed | tf_op | source)
XLA Modules:
  0.0 643.3 jit_solution(78488061301699797)
XLA Ops:
  7.7 2.1 bitcast_add_fusion.1
  10.3 1.7 reshape.106
  14.8 2.4 exponential_multiply_fusion.3
  17.2 1.3 fusion.7
  18.6 2.0 fusion.6
  22.6 44.0 %all_gather.38 = bf16[16,4,128]{2,1,0:T(4,128)(2,1)} all-gather(bf16[1,4,128]{2,1,0:T(4,128)(2,1)S(1)} %slice.20), channel_id=1, replica_groups=mesh['sp'=16,'tp'=2] {'sp'}, dimensions={0}, use_global_device_ids=true | all-gather | bytes 17408 | tf_op jit(solution)/shard_map/all_gather | solution.py:19
  66.7 35.8 %all_gather.35 = bf16[16,4,128]{2,1,0:T(4,128)(2,1)S(1)} all-gather(bf16[1,4,128]{2,1,0:T(4,128)(2,1)S(1)} %slice.21), channel_id=1, replica_groups=mesh['sp'=16,'tp'=2] {'sp'}, dimensions={0}, use_global_device_ids=true | all-gather | bytes 17408 | tf_op jit(solution)/shard_map/all_gather | solution.py:19
  102.5 1.6 convolution_multiply_fusion.2
  107.2 26.5 %while.17 = (s32[]{:T(128)}, f32[4,128,128]{2,1,0:T(8,128)S(1)}, s32[]{:T(128)}, bf16[16,4,128]{2,1,0:T(4,128)(2,1)}, bf16[16,4,128,128]{3,2,1,0:T(8,128)(2,1)},...) while((s32[]{:T(128)}, f32[4,128,128]{2,1,0:T(8,128)S(1)}, s32[]{:T(128)}, bf16[16,4,128]{2,1,0:T(4,128)(2,1)}, ...), condition=%wide.region_5.6_spmd, body=%wide.region_4.5_spmd.sunk | while | flops 197126 | bytes 660627 | solution.py:34
  133.6 1.3 fusion.1
  134.9 1.9 rev.20
  136.9 7.2 %all-gather.14.cloned.1.call-done = bf16[64,128,128]{2,1,0:T(8,128)(2,1)} async-done(((bf16[4,128,128]{2,1,0:T(8,128)(2,1)}), bf16[64,128,128]{2,1,0:T(8,128)(2,1)}) %all-gather.14.cloned.1.call-update) | async-done | bytes 2097168 | tf_op jit(solution)/shard_map/all_gather | solution.py:19
  145.7 2.0 all_gather.41
  148.3 2.5 all-reduce.1
  151.0 2.4 all_gather.42
  153.3 133.7 %all-gather.8.cloned.1.call-done = bf16[2048,2816]{1,0:T(8,128)(2,1)} async-done(((bf16[128,2816]{1,0:T(8,128)(2,1)}), bf16[2048,2816]{1,0:T(8,128)(2,1)}) %all-gather.8.cloned.1.call-update) | async-done | bytes 11534352 | tf_op jit(solution)/shard_map/all_gather | solution.py:116
  287.0 7.0 %fusion.40 = f32[128,2816]{1,0:T(8,128)} fusion(bf16[128,2048]{1,0:T(8,128)(2,1)S(1)} %all_gather.42, bf16[2048,2816]{1,0:T(8,128)(2,1)} %all-gather.8.cloned.1.call-done), kind=kOutput, calls=%fused_computation.91 | convolution fusion | flops 1476395008 | bytes 13500416 | tf_op jit(solution)/shard_map/dot_general | solution.py:179
  294.1 135.2 %all-gather.10.cloned.1.call-done = bf16[2048,2816]{1,0:T(8,128)(2,1)} async-done(((bf16[128,2816]{1,0:T(8,128)(2,1)}), bf16[2048,2816]{1,0:T(8,128)(2,1)}) %all-gather.10.cloned.1.call-update) | async-done | bytes 11534352 | tf_op jit(solution)/shard_map/all_gather | solution.py:117
  429.3 182.8 %all-gather.12.cloned.1.call-done = bf16[2816,2048]{1,0:T(8,128)(2,1)} async-done(((bf16[2816,128]{1,0:T(8,128)(2,1)}), bf16[2816,2048]{1,0:T(8,128)(2,1)}) %all-gather.12.cloned.1.call-update) | async-done | bytes 11534352 | tf_op jit(solution)/shard_map/all_gather | solution.py:118
  612.1 12.3 %convolution_convert_fusion = bf16[128,2048]{1,0:T(8,128)(2,1)} fusion(bf16[2816,2048]{1,0:T(8,128)(2,1)} %all-gather.12.cloned.1.call-done, bf16[128,2048]{1,0:T(8,128)(2,1)S(1)} %all_gather.42, bf16[2048,2816]{1,0:T(8,128)(2,1)} %all-gather.10.cloned.1.call-done, f32[128,2816]{1,0:T(8,128)} %fusion.40), kind=kOutput, calls=%fused_computation.6 | convolution fusion | flops 2955214848 | bytes 25559040 | tf_op jit(solution)/shard_map/dot_general | solution.py:182
  624.4 6.3 reduce-scatter.2.cloned.1.call-done
  630.7 1.3 fusion.8
  632.0 2.5 all-reduce
  634.5 1.9 add_convert_fusion
  (98 shorter events, 37.8 us)
Async XLA Ops:
  6.5 141.2 %copy-start = (bf16[1024,1024]{1,0:T(8,128)(2,1)S(1)}, bf16[1024,1024]{1,0:T(8,128)(2,1)}, u32[]{:S(2)}) copy-start(bf16[1024,1024]{1,0:T(8,128)(2,1)} %param.32) | copy-start | bytes 6291460
  6.5 100.6 %all-gather.16.cloned.1.call-start = ((), (), s32[]{:S(2)}) async-start(), calls=%async_computation.6 | async-start | bytes 2228224 | tf_op jit(solution)/shard_map/all_gather | solution.py:19
  9.8 4.8 copy-start.1
  9.9 2.1 copy-start.2
  18.5 125.5 %all-gather.14.cloned.1.call-start = ((), (), s32[]{:S(2)}) async-start(), calls=%async_computation.5 | async-start | bytes 2228224 | tf_op jit(solution)/shard_map/all_gather | solution.py:19
  20.6 266.4 %all-gather.8.cloned.1.call-start = ((), (), s32[]{:S(2)}) async-start(), calls=%async_computation.1 | async-start | bytes 12255232 | tf_op jit(solution)/shard_map/all_gather | solution.py:116
  21.4 407.9 %all-gather.10.cloned.1.call-start = ((), (), s32[]{:S(2)}) async-start(), calls=%async_computation.2 | async-start | bytes 12255232 | tf_op jit(solution)/shard_map/all_gather | solution.py:117
  22.0 590.1 %all-gather.12.cloned.1.call-start = ((), (), s32[]{:S(2)}) async-start(), calls=%async_computation.3 | async-start | bytes 12255232 | tf_op jit(solution)/shard_map/all_gather | solution.py:118
  22.5 608.2 %reduce-scatter.2.cloned.1.call-start = ((), (), s32[]{:S(2)}) async-start(), calls=%async_computation.4 | async-start | bytes 786432 | tf_op jit(solution)/shard_map/reduce_scatter | solution.py:183
  22.6 82.6 %copy-start.3 = (f32[128,4,128]{2,1,0:T(4,128)S(1)}, f32[128,4,128]{2,1,0:T(4,128)}, u32[]{:S(2)}) copy-start(f32[128,4,128]{2,1,0:T(4,128)} %get-tuple-element.229) | copy-start | bytes 786436
  144.1 1.5 copy-start.5
  144.1 3.7 copy-start.4
  145.6 5.2 copy-start.6
  145.6 5.2 copy-start.7
  294.1 340.4 %copy-start.8 = (f32[1024]{0:T(1024)S(1)}, f32[1024]{0:T(1024)}, u32[]{:S(2)}) copy-start(f32[1024]{0:T(1024)} %param.39) | copy-start | bytes 12292
  294.1 340.4 %copy-start.9 = (f32[1024]{0:T(1024)S(1)}, f32[1024]{0:T(1024)}, u32[]{:S(2)}) copy-start(f32[1024]{0:T(1024)} %param.38) | copy-start | bytes 12292
Sparse Core Ops, SparseCore 0:
  18.7 63.2 all-gather.15
  84.7 59.2 all-gather.13
  146.8 140.2 all-gather.7
  289.7 139.5 all-gather.9
  431.8 180.2 all-gather.11
  624.5 6.1 reduce-scatter.1
where the time goes:
time: 644 us; the launch traced here: 643 us
  waiting for transfers between devices  467 us (73%)
  blocking collectives  89.1 us (14%)
  other arithmetic  36 us (6%)
  matrix products  29.8 us (5%)
  between operations  13.7 us (2%)
  local copies, waits for them, and re-layouts  6.96 us (1%)
    all_gather x1, waiting for transfers between devices, shards(): lax.all_gather(down_matrix, 'sp', axis=1, tiled=True)  183 us
    all_gather x1, waiting for transfers between devices, shards(): lax.all_gather(up_matrix, 'sp', axis=0, tiled=True)  135 us
    all_gather x1, waiting for transfers between devices, shards(): lax.all_gather(gate_matrix, 'sp', axis=0, tiled=True)  134 us
    all_gather x2, blocking collectives, prefix(): lax.all_gather(a.astype(kind), axis)  79.8 us
    add x15, other arithmetic, join(): jnp.exp(later[0])[:, :, None] * earlier[1] + later[1]  16.1 us
  transfers between devices with their start and end apart: 6, of which 5 were waited for; matrix products, arithmetic and copies ran while one was open for 7% of the time, Pallas kernels for 0%

commit v1 on v0

--- a/solution.py
+++ b/solution.py
@@ -113,7 +113,15 @@
     closing_norm_bias,
 ):
     gate_whole, up_whole, down_whole = (
-        lax.all_gather(gate_matrix, "sp", axis=0, tiled=True),
+        jnp.concatenate(
+            lax.all_to_all(
+                jnp.stack([gate_matrix] * lax.axis_size("sp")),
+                axis_name="sp",
+                split_axis=0,
+                concat_axis=0,
+            ),
+            axis=0,
+        ),
         lax.all_gather(up_matrix, "sp", axis=0, tiled=True),
         lax.all_gather(down_matrix, "sp", axis=1, tiled=True),
     )

time: 644 us -> 706 us (1.096)
  blocking collectives: 89.1 us -> 345 us
  waiting for transfers between devices: 467 us -> 258 us
  starting transfers between devices: 0.2 us -> 8.55 us
    all_gather x2, blocking collectives: 79.8 us -> 335 us  [prefix(): lax.all_gather(a.astype(kind), axis)]
    all_gather x1 -> x0, waiting for transfers between devices: 134 us -> none  [shards(): lax.all_gather(gate_matrix, 'sp', axis=0, tiled=True)]
    all_gather x1, waiting for transfers between devices: 135 us -> 67.5 us  [shards(): lax.all_gather(up_matrix, 'sp', axis=0, tiled=True)]
    all_to_all x0 -> x1, starting transfers between devices: none -> 8.39 us  [shards(): lax.all_to_all(jnp.stack([gate_matrix] * lax.axis_size('sp')), axis_name=...]
    all_gather x2, waiting for transfers between devices: 7.19 us -> 0.04 us  [prefix(): lax.all_gather(a.astype(kind), axis)]
  transfers between devices with their start and end apart: 6 -> 6, of which waited for: 5 -> 3; matrix products, arithmetic and copies ran while one was open for 7% -> 7% of each run, Pallas kernels for 0% -> 0%
where the time goes in v1:
time: 706 us; the launch traced here: 704 us
  blocking collectives  345 us (49%)
  waiting for transfers between devices  258 us (37%)
  other arithmetic  36 us (5%)
  matrix products  29.9 us (4%)
  between operations  13.4 us (2%)
  local copies, waits for them, and re-layouts  13.3 us (2%)
  starting transfers between devices  8.55 us (1%)
    all_gather x2, blocking collectives, prefix(): lax.all_gather(a.astype(kind), axis)  335 us
    all_gather x1, waiting for transfers between devices, shards(): lax.all_gather(down_matrix, 'sp', axis=1, tiled=True)  183 us
    all_gather x1, waiting for transfers between devices, shards(): lax.all_gather(up_matrix, 'sp', axis=0, tiled=True)  67.5 us
    add x15, other arithmetic, join(): jnp.exp(later[0])[:, :, None] * earlier[1] + later[1]  16.1 us
  transfers between devices with their start and end apart: 6, of which 3 were waited for; matrix products, arithmetic and copies ran while one was open for 7% of the time, Pallas kernels for 0%

profile of v1, /device:TPU:0, one launch (start us, length us, event | category | flops | bytes accessed | tf_op | source)
XLA Modules:
  0.0 704.4 jit_solution(14386993924600513553)
XLA Ops:
  7.7 2.0 bitcast_add_fusion.1
  10.2 1.7 reshape.111
  14.7 2.4 exponential_multiply_fusion.3
  17.1 1.3 fusion.7
  18.5 2.0 fusion.6
  21.2 6.4 stack.2
  27.6 8.4 %all-to-all-start = ((bf16[16,128,2816]{2,1,0:T(8,128)(2,1)}), bf16[16,128,2816]{2,1,0:T(8,128)(2,1)}, u32[]{:S(2)}, u32[]{:S(2)}) async-start(bf16[16,128,2816]{2,1,0:T(8,128)(2,1)} %stack.2), calls=%async_computation | async-start | bytes 23068672 | tf_op jit(solution)/shard_map/all_to_all | solution.py:117
  36.7 257.1 %all_gather.35 = bf16[16,4,128]{2,1,0:T(4,128)(2,1)} all-gather(bf16[1,4,128]{2,1,0:T(4,128)(2,1)S(1)} %slice.20), channel_id=1, replica_groups=mesh['sp'=16,'tp'=2] {'sp'}, dimensions={0}, use_global_device_ids=true | all-gather | bytes 17408 | tf_op jit(solution)/shard_map/all_gather | solution.py:19
  293.8 78.4 %all_gather.32 = bf16[16,4,128]{2,1,0:T(4,128)(2,1)S(1)} all-gather(bf16[1,4,128]{2,1,0:T(4,128)(2,1)S(1)} %slice.21), channel_id=1, replica_groups=mesh['sp'=16,'tp'=2] {'sp'}, dimensions={0}, use_global_device_ids=true | all-gather | bytes 17408 | tf_op jit(solution)/shard_map/all_gather | solution.py:19
  372.2 1.6 convolution_multiply_fusion.2
  376.9 26.5 %while.17 = (s32[]{:T(128)}, f32[4,128,128]{2,1,0:T(8,128)S(1)}, s32[]{:T(128)}, bf16[16,4,128]{2,1,0:T(4,128)(2,1)}, bf16[16,4,128,128]{3,2,1,0:T(8,128)(2,1)},...) while((s32[]{:T(128)}, f32[4,128,128]{2,1,0:T(8,128)S(1)}, s32[]{:T(128)}, bf16[16,4,128]{2,1,0:T(4,128)(2,1)}, ...), condition=%wide.region_5.6_spmd, body=%wide.region_4.5_spmd.sunk | while | flops 197126 | bytes 660627 | solution.py:34
  403.4 1.3 fusion.1
  404.7 1.9 rev.20
  408.4 2.0 all_gather.38
  411.0 2.5 all-reduce.1
  413.6 2.4 all_gather.39
  416.0 7.1 %fusion.40 = f32[128,2816]{1,0:T(8,128)} fusion(bf16[128,2048]{1,0:T(8,128)(2,1)S(1)} %all_gather.39, bf16[2048,2816]{1,0:T(8,128)(2,1)} %bitcast.15), kind=kOutput, calls=%fused_computation.91 | convolution fusion | flops 1476395008 | bytes 13500416 | tf_op jit(solution)/shard_map/dot_general | solution.py:187
  423.1 67.5 %all-gather.7.cloned.1.call-done = bf16[2048,2816]{1,0:T(8,128)(2,1)} async-done(((bf16[128,2816]{1,0:T(8,128)(2,1)}), bf16[2048,2816]{1,0:T(8,128)(2,1)}) %all-gather.7.cloned.1.call-update) | async-done | bytes 11534352 | tf_op jit(solution)/shard_map/all_gather | solution.py:125
  490.6 182.8 %all-gather.9.cloned.1.call-done = bf16[2816,2048]{1,0:T(8,128)(2,1)} async-done(((bf16[2816,128]{1,0:T(8,128)(2,1)}), bf16[2816,2048]{1,0:T(8,128)(2,1)}) %all-gather.9.cloned.1.call-update) | async-done | bytes 11534352 | tf_op jit(solution)/shard_map/all_gather | solution.py:126
  673.4 12.5 %convolution_convert_fusion = bf16[128,2048]{1,0:T(8,128)(2,1)} fusion(bf16[2816,2048]{1,0:T(8,128)(2,1)} %all-gather.9.cloned.1.call-done, bf16[128,2048]{1,0:T(8,128)(2,1)S(1)} %all_gather.39, bf16[2048,2816]{1,0:T(8,128)(2,1)} %all-gather.7.cloned.1.call-done, f32[128,2816]{1,0:T(8,128)} %fusion.40), kind=kOutput, calls=%fused_computation.6 | convolution fusion | flops 2955214848 | bytes 25559040 | tf_op jit(solution)/shard_map/dot_general | solution.py:190
  685.9 6.3 reduce-scatter.2.cloned.1.call-done
  692.1 1.3 fusion.8
  693.4 2.5 all-reduce
  695.9 1.9 add_convert_fusion
  (98 shorter events, 37.3 us)
Async XLA Ops:
  6.5 403.9 %copy-start = (bf16[1024,1024]{1,0:T(8,128)(2,1)S(1)}, bf16[1024,1024]{1,0:T(8,128)(2,1)}, u32[]{:S(2)}) copy-start(bf16[1024,1024]{1,0:T(8,128)(2,1)} %param.32) | copy-start | bytes 6291460
  6.5 370.3 %all-gather.13.cloned.1.call-start = ((), (), s32[]{:S(2)}) async-start(), calls=%async_computation.6 | async-start | bytes 2228224 | tf_op jit(solution)/shard_map/all_gather | solution.py:19
  9.8 4.8 copy-start.2
  18.4 388.3 %all-gather.11.cloned.1.call-start = ((), (), s32[]{:S(2)}) async-start(), calls=%async_computation.5 | async-start | bytes 2228224 | tf_op jit(solution)/shard_map/all_gather | solution.py:19
  20.5 470.1 %all-gather.7.cloned.1.call-start = ((), (), s32[]{:S(2)}) async-start(), calls=%async_computation.2 | async-start | bytes 12255232 | tf_op jit(solution)/shard_map/all_gather | solution.py:125
  27.6 388.4 %all-to-all-start = ((bf16[16,128,2816]{2,1,0:T(8,128)(2,1)}), bf16[16,128,2816]{2,1,0:T(8,128)(2,1)}, u32[]{:S(2)}, u32[]{:S(2)}) async-start(bf16[16,128,2816]{2,1,0:T(8,128)(2,1)} %stack.2), calls=%async_computation | async-start | bytes 23068672 | tf_op jit(solution)/shard_map/all_to_all | solution.py:117
  36.0 637.4 %all-gather.9.cloned.1.call-start = ((), (), s32[]{:S(2)}) async-start(), calls=%async_computation.3 | async-start | bytes 12255232 | tf_op jit(solution)/shard_map/all_gather | solution.py:126
  36.6 655.5 %reduce-scatter.2.cloned.1.call-start = ((), (), s32[]{:S(2)}) async-start(), calls=%async_computation.4 | async-start | bytes 786432 | tf_op jit(solution)/shard_map/reduce_scatter | solution.py:191
  36.7 338.2 %copy-start.3 = (f32[128,4,128]{2,1,0:T(4,128)S(1)}, f32[128,4,128]{2,1,0:T(4,128)}, u32[]{:S(2)}) copy-start(f32[128,4,128]{2,1,0:T(4,128)} %get-tuple-element.229) | copy-start | bytes 786436
  406.7 1.5 copy-start.5
  406.7 3.7 copy-start.4
  408.3 5.2 copy-start.6
  408.3 5.2 copy-start.7
  423.1 272.8 %copy-start.8 = (f32[1024]{0:T(1024)S(1)}, f32[1024]{0:T(1024)}, u32[]{:S(2)}) copy-start(f32[1024]{0:T(1024)} %param.39) | copy-start | bytes 12292
  423.1 272.8 %copy-start.9 = (f32[1024]{0:T(1024)S(1)}, f32[1024]{0:T(1024)}, u32[]{:S(2)}) copy-start(f32[1024]{0:T(1024)} %param.38) | copy-start | bytes 12292
  673.4 24.4 %copy-start.1 = (bf16[1024,1024]{1,0:T(8,128)(2,1)S(1)}, bf16[1024,1024]{1,0:T(8,128)(2,1)}, u32[]{:S(2)}) copy-start(bf16[1024,1024]{1,0:T(8,128)(2,1)} %param.32) | copy-start | bytes 6291460
Sparse Core Ops, SparseCore 0:
  18.5 244.7 all-gather.12
  266.1 81.4 all-gather.10
  350.4 140.1 all-gather.6
  493.1 180.2 all-gather.8
  686.0 6.0 reduce-scatter.1
